TPU v7x, 32 devices: a whole 2x2x4 slice. The times are simulated.
32 devices in a mesh: sp: 16 (over z, y, x), tp: 2 (over core).
Axes of the slice: x: 2, y: 2, z: 4, core: 2. Of those that a mesh axis runs over, the one named last changes fastest.
Arguments:
- tokens: bfloat16 [4096, 2048], P('sp'), may hold values from -6 to 6
- input_norm_gain: float32 [2048], replicated, may hold values from 0.1 to 1.9
- query_matrix: bfloat16 [2048, 1024], P('sp', 'tp'), may hold values from -0.125 to 0.125
- key_matrix: bfloat16 [2048, 1024], P('sp', 'tp'), may hold values from -0.125 to 0.125
- value_matrix: bfloat16 [2048, 1024], P('sp', 'tp'), may hold values from -0.125 to 0.125
- convolution_value_matrix: bfloat16 [2048, 2048], P('sp', 'tp'), may hold values from -0.125 to 0.125
- convolution_gate_matrix: bfloat16 [2048, 2048], P('sp', 'tp'), may hold values from -0.125 to 0.125
- decay_offset_channel: float32 [1024], P('tp'), may hold values from -16 to -2
- decay_first_matrix: bfloat16 [2048, 128], replicated, may hold values from -0.125 to 0.125
- decay_second_matrix: bfloat16 [128, 1024], P(None, 'tp'), may hold values from -0.59765625 to 0.59765625
- learning_rate_offset: float32 [1024], P('tp'), may hold values from -9 to 1
- learning_rate_first_matrix: bfloat16 [2048, 128], replicated, may hold values from -0.125 to 0.125
- learning_rate_second_matrix: bfloat16 [128, 1024], P(None, 'tp'), may hold values from -0.5 to 0.5
- forgetting_rate_factor: float32 [4096, 16], P('sp', 'tp'), may hold values from 0.39 to 2.53
- state_retention_share: float32 [4096, 16], P('sp', 'tp'), may hold values from 0.12 to 1
- per_head_norm_gain: float32 [1024], P('tp'), may hold values from 0.1 to 1.9
- convolution_filter_taps: float32 [31, 2048], P(None, 'tp'), may hold values from -81 to 81
- convolution_channel_gain: float32 [2048], P('tp'), may hold values from 0.1 to 1.9
- attention_output_matrix: bfloat16 [2048, 1024], P('sp', 'tp'), may hold values from -0.109375 to 0.109375
- convolution_output_matrix: bfloat16 [2048, 2048], P('sp', 'tp'), may hold values from -0.109375 to 0.109375
Outputs:
- mixed: bfloat16 [4096, 2048], P('sp')
All inputs are finite; a program needn't handle non-finite values.
Results may differ from a plain program's by a relative error of at most 0.014.
Values may be sent and summed in bfloat16 or wider, within the bound.
A program may use at most 128 MiB of HBM per device.

v0:
```python
import math
import jax
import jax.numpy as jnp
from jax import lax
from jax.sharding import PartitionSpec as P

CONV_CH = 2048
HIGHEST = lax.Precision.HIGHEST
RMS_EPSILON = 1e-06
GROUP_EPSILON = 0.00064
LAYER_EPSILON = 1e-05
UNIT_EPSILON = 1e-06


def entering(x, axis, combine, identity):
    count, place = (lax.axis_size(axis), lax.axis_index(axis))
    everything = jax.tree.map(lambda part: lax.all_gather(part, axis), x)
    start = jax.tree.map(
        lambda part, zero: jnp.broadcast_to(jnp.asarray(zero, part.dtype), part.shape), x, identity
    )

    def hop(k, before):
        reached = k < place
        new = combine(before, jax.tree.map(lambda part: part[k], everything))
        return jax.tree.map(lambda a, b: jnp.where(reached, a, b), new, before)

    return lax.fori_loop(0, count, hop, start)


def from_behind(value, axis, steps):
    count = lax.axis_size(axis)
    initial, last = (max(0, -steps), min(count, count - steps))
    return lax.ppermute(value, axis, [(source, source + steps) for source in range(initial, last)])


def exact_mul(form, left, right):
    return jnp.einsum(form, left, right, precision=HIGHEST)


def chain_pair(earlier, later):
    return (
        exact_mul("...cd,...de->...ce", earlier[0], later[0]),
        exact_mul("...vd,...de->...ve", earlier[1], later[0]) + later[1],
    )


def split_blocks(values, block_count, block_len):
    return values.reshape((block_count, block_len) + values.shape[1:]).transpose(0, 2, 1, 3)


def block_update(carry, inputs):
    phi_sofar, psi_sofar = carry
    query_blk, logdec_blk, key_blk, value_blk, erase_blk, write_blk = inputs
    block_len = query_blk.shape[1]
    head_size = query_blk.shape[2]
    log_gain = jnp.cumsum(logdec_blk, axis=1)
    log_before = log_gain - logdec_blk
    positions = jnp.arange(block_len)
    strict = positions[:, None] > positions[None, :]
    pair_decay = jnp.exp(
        jnp.where(
            strict[None, :, :, None], log_before[:, :, None, :] - log_gain[:, None, :, :], -jnp.inf
        )
    )

    def paired(left, right):
        return jnp.einsum("htc,htsc,hsc->hts", left, pair_decay, right, precision=HIGHEST)

    step_query = query_blk * jnp.exp(logdec_blk)
    identity_blk = jnp.eye(block_len, dtype=jnp.float32)
    erase_write = paired(erase_blk, write_blk)
    erase_key = paired(erase_blk, key_blk)
    read_write = (
        paired(step_query, write_blk)
        + identity_blk * jnp.sum(query_blk * write_blk, axis=-1)[:, :, None]
    )
    read_key = (
        paired(step_query, key_blk)
        + identity_blk * jnp.sum(query_blk * key_blk, axis=-1)[:, :, None]
    )
    inverse = identity_blk + erase_write
    power = erase_write
    for level in range(block_len.bit_length() - 2):
        power = exact_mul("hts,hsu->htu", power, power)
        inverse = inverse + exact_mul("hts,hsu->htu", inverse, power)
    erase_hat = erase_blk * jnp.exp(log_before)
    query_hat = query_blk * jnp.exp(log_gain)
    total_gain = log_gain[:, -1:, :]
    to_end = jnp.exp(total_gain - log_gain)
    write_end = write_blk * to_end
    key_end = key_blk * to_end
    pulled = exact_mul("hts,hsv->htv", inverse, exact_mul("hts,hsv->htv", erase_key, value_blk))
    local_out = exact_mul("hts,hsv->htv", read_write, pulled) + exact_mul(
        "hts,hsv->htv", read_key, value_blk
    )
    psi_block = exact_mul("hsv,hsc->hvc", pulled, write_end) + exact_mul(
        "hsv,hsc->hvc", value_blk, key_end
    )
    erase_solved = exact_mul("hts,hsc->htc", inverse, erase_hat)
    query_full = query_hat + exact_mul("hts,hsc->htc", read_write, erase_solved)
    identity_key = jnp.eye(head_size, dtype=jnp.float32)
    phi_block = jnp.exp(total_gain[:, 0, :])[:, :, None] * identity_key + exact_mul(
        "hsc,hsd->hcd", erase_solved, write_end
    )
    local_out = local_out + exact_mul("htc,hvc->htv", query_full, psi_sofar)
    carried_query = exact_mul("htc,hdc->htd", query_full, phi_sofar)
    phi_next = exact_mul("hcd,hde->hce", phi_sofar, phi_block)
    psi_next = exact_mul("hvd,hde->hve", psi_sofar, phi_block) + psi_block
    return ((phi_next, psi_next), (local_out, carried_query))


def body(
    tokens,
    input_norm_gain,
    query_matrix,
    key_matrix,
    value_matrix,
    convolution_value_matrix,
    convolution_gate_matrix,
    decay_offset_channel,
    decay_first_matrix,
    decay_second_matrix,
    learning_rate_offset,
    learning_rate_first_matrix,
    learning_rate_second_matrix,
    forgetting_rate_factor,
    state_retention_share,
    per_head_norm_gain,
    convolution_filter_taps,
    convolution_channel_gain,
    attention_output_matrix,
    convolution_output_matrix,
):
    tok_rows = tokens.shape[0]
    heads_dev = forgetting_rate_factor.shape[1]
    head_size = query_matrix.shape[1] // heads_dev
    widened = tokens.astype(jnp.float32)
    normed = (
        widened
        * lax.rsqrt(jnp.mean(widened * widened, axis=-1, keepdims=True) + RMS_EPSILON)
        * input_norm_gain
    ).astype(jnp.bfloat16)
    pieces = (
        lax.all_gather(query_matrix, "sp", axis=0, tiled=True),
        lax.all_gather(key_matrix, "sp", axis=0, tiled=True),
        lax.all_gather(value_matrix, "sp", axis=0, tiled=True),
        lax.all_gather(convolution_value_matrix, "sp", axis=0, tiled=True),
        lax.all_gather(convolution_gate_matrix, "sp", axis=0, tiled=True),
    )
    query_proj, key_proj, value_proj, conv_value, conv_gate = tuple(
        (jnp.dot(normed, piece, preferred_element_type=jnp.float32) for piece in pieces)
    )
    decay_mid = jnp.tanh(
        jnp.dot(normed, decay_first_matrix, preferred_element_type=jnp.float32)
    ).astype(jnp.bfloat16)
    rate_mid = jnp.dot(
        normed, learning_rate_first_matrix, preferred_element_type=jnp.float32
    ).astype(jnp.bfloat16)
    logarithm_learning_rate = (
        -jax.nn.softplus(
            -(
                decay_offset_channel
                + jnp.dot(decay_mid, decay_second_matrix, preferred_element_type=jnp.float32)
            )
        )
        - 0.5
    )
    learn_rate = jax.nn.sigmoid(
        learning_rate_offset
        + jnp.dot(rate_mid, learning_rate_second_matrix, preferred_element_type=jnp.float32)
    )
    reshaped_tensor = (tok_rows, heads_dev, head_size)
    log_decay = (
        -jnp.exp(logarithm_learning_rate).reshape(reshaped_tensor)
        * forgetting_rate_factor[:, :, None]
        + jnp.log(state_retention_share)[:, :, None]
    )
    key_heads = key_proj.reshape(reshaped_tensor)
    unit_key = key_heads * lax.rsqrt(
        jnp.sum(key_heads * key_heads, axis=-1, keepdims=True) + UNIT_EPSILON
    )
    erase = -unit_key
    write = unit_key * learn_rate.reshape(reshaped_tensor)
    block_len = math.gcd(tok_rows, 128)
    block_count = tok_rows // block_len
    inputs = tuple(
        (
            split_blocks(item, block_count, block_len)
            for item in (
                query_proj.reshape(reshaped_tensor),
                log_decay,
                key_heads,
                value_proj.reshape(reshaped_tensor),
                erase,
                write,
            )
        )
    )
    identity_key = jnp.broadcast_to(
        jnp.eye(head_size, dtype=jnp.float32), (heads_dev, head_size, head_size)
    )
    device_pair, block_outs = lax.scan(
        block_update, (identity_key, jnp.zeros_like(identity_key)), inputs
    )
    local_out, carried_query = block_outs
    phi_device, psi_device = device_pair
    prefix = entering(
        (phi_device, psi_device), "sp", chain_pair, (identity_key, jnp.zeros_like(identity_key))
    )
    state_in = prefix[1]
    state_out = local_out + exact_mul("bhtd,hvd->bhtv", carried_query, state_in)
    state_rows = state_out.transpose(0, 2, 1, 3).reshape(reshaped_tensor)
    centred = state_rows - jnp.mean(state_rows, axis=-1, keepdims=True)
    normal_state = centred * lax.rsqrt(
        jnp.mean(centred * centred, axis=-1, keepdims=True) + GROUP_EPSILON
    )
    state_mixed = (
        (normal_state * per_head_norm_gain.reshape(heads_dev, head_size))
        .reshape(tok_rows, heads_dev * head_size)
        .astype(jnp.bfloat16)
    )
    gated = (conv_value * jax.nn.sigmoid(conv_gate)).astype(jnp.bfloat16)
    span = convolution_filter_taps.shape[0]
    rim = from_behind(gated[tok_rows - (span - 1) :], "sp", 1)
    padded = jnp.concatenate([rim, gated], axis=0)
    filtered = jnp.zeros(gated.shape, jnp.float32)
    for offset in range(span):
        filtered = filtered + convolution_filter_taps[offset] * padded[offset : offset + tok_rows]
    total_sum, total_square = lax.psum(
        (jnp.sum(filtered, axis=-1), jnp.sum(filtered * filtered, axis=-1)), "tp"
    )
    row_mean = total_sum / CONV_CH
    deviation = filtered - row_mean[:, None]
    variance = total_square / CONV_CH - row_mean * row_mean
    conv_mixed = jax.nn.silu(
        deviation * lax.rsqrt(variance + LAYER_EPSILON)[:, None] * convolution_channel_gain
    ).astype(jnp.bfloat16)
    contract_dims = (((1,), (1,)), ((), ()))
    pieces = lax.all_gather(
        (attention_output_matrix, convolution_output_matrix), "sp", axis=0, tiled=True
    )
    partial_out = lax.dot_general(
        state_mixed, pieces[0], contract_dims, preferred_element_type=jnp.float32
    ) + lax.dot_general(conv_mixed, pieces[1], contract_dims, preferred_element_type=jnp.float32)
    return lax.psum(partial_out.astype(jnp.bfloat16), "tp")


def solution(mesh):
    return jax.shard_map(
        body,
        mesh=mesh,
        in_specs=(
            P("sp", None),
            P(),
            P("sp", "tp"),
            P("sp", "tp"),
            P("sp", "tp"),
            P("sp", "tp"),
            P("sp", "tp"),
            P("tp"),
            P(),
            P(None, "tp"),
            P("tp"),
            P(),
            P(None, "tp"),
            P("sp", "tp"),
            P("sp", "tp"),
            P("tp"),
            P(None, "tp"),
            P("tp"),
            P("sp", "tp"),
            P("sp", "tp"),
        ),
        out_specs=P("sp", None),
        check_vma=False,
    )
```

profile of v0, /device:TPU:0, one launch (start us, length us, event | category | flops | bytes accessed | tf_op | source)
XLA Modules:
  0.0 1069.4 jit_solution(5047170836986482139)
XLA Ops:
  17.3 55.9 %all-gather.12.cloned.1.call-done = bf16[2048,512]{1,0:T(8,128)(2,1)} async-done(((bf16[128,512]{1,0:T(8,128)(2,1)}), bf16[2048,512]{1,0:T(8,128)(2,1)}) %all-gather.12.cloned.1.call-update) | async-done | bytes 2097168 | tf_op jit(solution)/shard_map/all_gather | solution.py:145
  77.1 58.1 %all-gather.14.cloned.1.call-done = bf16[2048,512]{1,0:T(8,128)(2,1)} async-done(((bf16[128,512]{1,0:T(8,128)(2,1)}), bf16[2048,512]{1,0:T(8,128)(2,1)}) %all-gather.14.cloned.1.call-update) | async-done | bytes 2097168 | tf_op jit(solution)/shard_map/all_gather | solution.py:146
  135.2 2.6 fusion.147
  138.1 59.1 %all-gather.16.cloned.1.call-done = bf16[2048,512]{1,0:T(8,128)(2,1)} async-done(((bf16[128,512]{1,0:T(8,128)(2,1)}), bf16[2048,512]{1,0:T(8,128)(2,1)}) %all-gather.16.cloned.1.call-update) | async-done | bytes 2097168 | tf_op jit(solution)/shard_map/all_gather | solution.py:144
  197.2 2.6 fusion.145
  200.9 2.6 multiply_bitcast_fusion.1
  204.2 387.9 %while.31 = (s32[]{:T(128)}, f32[8,64,64]{1,2,0:T(8,128)}, f32[8,64,64]{1,2,0:T(8,128)S(1)}, f32[2,8,128,64]{2,3,0,1:T(8,128)}, f32[2,8,128,64]{2,3,0,1:T(8,128)...) while((s32[]{:T(128)}, f32[8,64,64]{1,2,0:T(8,128)}, ...), condition=%wide.region_6.7_spmd.clone, body=%wide.region_2.6_spmd.clone.sunk | while | flops 3836598272 | bytes 58414024 | solution.py:202
  206.6 23.3 %fusion.369 = f32[8,128,64]{2,0,1:T(8,128)S(1)} fusion(f32[8,128,64]{2,0,1:T(8,128)S(1)} %copy.214), kind=kOutput, calls=%fused_computation.245.clone.1 | output fusion | flops 8323072 | bytes 524288 | tf_op jit(solution)/shard_map/while/body/eval_jaxpr/jit(cumsum)/reduce_window_sum | solution.py:56
  235.5 33.2 %fusion.370 = f32[8,128,1,128]{3,2,1,0:T(1,128)S(1)} fusion(f32[8,128,64,1]{2,3,1,0:T(1,128)} %copy.213, f32[8,128,64]{1,2,0:T(8,128)S(1)} %bitcast.376, f32[8,128,64]{1,2,0:T(8,128)S(1)} %copy.215, f32[8,128,64]{2,1,0:T(8,128)S(1)} %copy.216, pred[128,128]{1,0:T(8,128)(4,1)S(1)} %iota_compare_fusion.5), kind=kOutput, calls=%fused_computation.6.clone.1 | convolution fusion | flops 125829120 | bytes 1589248 | tf_op jit(solution)/shard_map/while/body/eval_jaxpr/htc,htsc,hsc->hts/dot_general | solution.py:67
  276.7 35.6 %fusion.381 = f32[8,128,1,128]{3,2,1,0:T(1,128)S(1)} fusion(f32[8,128,64,1]{2,3,1,0:T(1,128)S(1)} %copy-done.6, f32[8,128,64]{1,2,0:T(8,128)S(1)} %bitcast.390, f32[8,128,64]{1,2,0:T(8,128)S(1)} %copy.215, f32[8,128,64]{2,1,0:T(8,128)S(1)} %copy-done.4, pred[128,128]{1,0:T(8,128)(4,1)S(1)} %iota_compare_fusion.5), kind=kOutput, calls=%fused_computation.2.clone.1 | convolution fusion | flops 125829120 | bytes 1589248 | tf_op jit(solution)/shard_map/while/body/eval_jaxpr/htc,htsc,hsc->hts/dot_general | solution.py:67
  317.8 33.1 %fusion.386 = f32[8,128,1,128]{3,2,1,0:T(1,128)S(1)} fusion(f32[8,128,64,1]{2,3,1,0:T(1,128)} %copy.217, f32[8,128,64]{1,2,0:T(8,128)S(1)} %bitcast.378, f32[8,128,64]{1,2,0:T(8,128)S(1)} %copy.215, f32[8,128,64]{2,1,0:T(8,128)} %copy-done.3, pred[128,128]{1,0:T(8,128)(4,1)S(1)} %iota_compare_fusion.5), kind=kOutput, calls=%fused_computation.4.clone.1 | convolution fusion | flops 125829120 | bytes 1589248 | tf_op jit(solution)/shard_map/while/body/eval_jaxpr/htc,htsc,hsc->hts/dot_general | solution.py:67
  352.0 31.7 %fusion.388 = f32[8,128,1,128]{3,2,1,0:T(1,128)S(1)} fusion(f32[8,128,64,1]{2,3,1,0:T(1,128)S(1)} %copy-done.7, f32[8,128,64]{1,2,0:T(8,128)S(1)} %bitcast.391, f32[8,128,64]{1,2,0:T(8,128)S(1)} %copy.215, f32[8,128,64]{2,1,0:T(8,128)S(1)} %copy-done.5, pred[128,128]{1,0:T(8,128)(4,1)S(1)} %iota_compare_fusion.5), kind=kOutput, calls=%fused_computation.clone.2 | convolution fusion | flops 125829120 | bytes 1589248 | tf_op jit(solution)/shard_map/while/body/eval_jaxpr/htc,htsc,hsc->hts/dot_general | solution.py:67
  397.4 23.3 %fusion.369 = f32[8,128,64]{2,0,1:T(8,128)S(1)} fusion(f32[8,128,64]{2,0,1:T(8,128)S(1)} %copy.214), kind=kOutput, calls=%fused_computation.245.clone.1 | output fusion | flops 8323072 | bytes 524288 | tf_op jit(solution)/shard_map/while/body/eval_jaxpr/jit(cumsum)/reduce_window_sum | solution.py:56
  426.4 33.0 %fusion.370 = f32[8,128,1,128]{3,2,1,0:T(1,128)S(1)} fusion(f32[8,128,64,1]{2,3,1,0:T(1,128)} %copy.213, f32[8,128,64]{1,2,0:T(8,128)S(1)} %bitcast.376, f32[8,128,64]{1,2,0:T(8,128)S(1)} %copy.215, f32[8,128,64]{2,1,0:T(8,128)S(1)} %copy.216, pred[128,128]{1,0:T(8,128)(4,1)S(1)} %iota_compare_fusion.5), kind=kOutput, calls=%fused_computation.6.clone.1 | convolution fusion | flops 125829120 | bytes 1589248 | tf_op jit(solution)/shard_map/while/body/eval_jaxpr/htc,htsc,hsc->hts/dot_general | solution.py:67
  467.4 35.6 %fusion.381 = f32[8,128,1,128]{3,2,1,0:T(1,128)S(1)} fusion(f32[8,128,64,1]{2,3,1,0:T(1,128)S(1)} %copy-done.6, f32[8,128,64]{1,2,0:T(8,128)S(1)} %bitcast.390, f32[8,128,64]{1,2,0:T(8,128)S(1)} %copy.215, f32[8,128,64]{2,1,0:T(8,128)S(1)} %copy-done.4, pred[128,128]{1,0:T(8,128)(4,1)S(1)} %iota_compare_fusion.5), kind=kOutput, calls=%fused_computation.2.clone.1 | convolution fusion | flops 125829120 | bytes 1589248 | tf_op jit(solution)/shard_map/while/body/eval_jaxpr/htc,htsc,hsc->hts/dot_general | solution.py:67
  508.5 33.1 %fusion.386 = f32[8,128,1,128]{3,2,1,0:T(1,128)S(1)} fusion(f32[8,128,64,1]{2,3,1,0:T(1,128)} %copy.217, f32[8,128,64]{1,2,0:T(8,128)S(1)} %bitcast.378, f32[8,128,64]{1,2,0:T(8,128)S(1)} %copy.215, f32[8,128,64]{2,1,0:T(8,128)} %copy-done.3, pred[128,128]{1,0:T(8,128)(4,1)S(1)} %iota_compare_fusion.5), kind=kOutput, calls=%fused_computation.4.clone.1 | convolution fusion | flops 125829120 | bytes 1589248 | tf_op jit(solution)/shard_map/while/body/eval_jaxpr/htc,htsc,hsc->hts/dot_general | solution.py:67
  542.7 31.7 %fusion.388 = f32[8,128,1,128]{3,2,1,0:T(1,128)S(1)} fusion(f32[8,128,64,1]{2,3,1,0:T(1,128)S(1)} %copy-done.7, f32[8,128,64]{1,2,0:T(8,128)S(1)} %bitcast.391, f32[8,128,64]{1,2,0:T(8,128)S(1)} %copy.215, f32[8,128,64]{2,1,0:T(8,128)S(1)} %copy-done.5, pred[128,128]{1,0:T(8,128)(4,1)S(1)} %iota_compare_fusion.5), kind=kOutput, calls=%fused_computation.clone.2 | convolution fusion | flops 125829120 | bytes 1589248 | tf_op jit(solution)/shard_map/while/body/eval_jaxpr/htc,htsc,hsc->hts/dot_general | solution.py:67
  597.9 70.6 %all-gather.26.cloned.1.call-done = f32[128,64,64]{2,1,0:T(8,128)} async-done(((f32[8,64,64]{2,1,0:T(8,128)}), f32[128,64,64]{2,1,0:T(8,128)}) %all-gather.26.cloned.1.call-update) | async-done | bytes 2097168 | tf_op jit(solution)/shard_map/all_gather | solution.py:17
  668.5 76.8 %all-gather.28.cloned.1.call-done = f32[128,64,64]{2,1,0:T(8,128)} async-done(((f32[8,64,64]{2,1,0:T(8,128)}), f32[128,64,64]{2,1,0:T(8,128)}) %all-gather.28.cloned.1.call-update) | async-done | bytes 2097168 | tf_op jit(solution)/shard_map/all_gather | solution.py:17
  745.4 43.6 %while.32 = (s32[]{:T(128)}, f32[8,64,64]{1,2,0:T(8,128)S(1)}, s32[]{:T(128)}, f32[16,8,64,64]{3,2,1,0:T(8,128)}, f32[16,8,64,64]{3,2,1,0:T(8,128)}, /*index=5*/s32[]{:T(128)}, s32[]{:T(128)}) while((s32[]{:T(128)}, f32[8,64,64]{1,2,0:T(8,128)S(1)}, s32[]{:T(128)}, f32[16,8,64,64]{3,2,1,0:T(8,128)}, f32[16,8,64,64]{3,2,1,0:T(8,128)}, ...), condition=%wide.region_8.9_spmd.clone, body=%wide.region_7.8_spmd.clone.sunk | while | flops 25296900 | bytes 1968227 | solution.py:27
  789.0 33.2 %all-gather.22.cloned.1.call-done = bf16[2048,1024]{1,0:T(8,128)(2,1)} async-done(((bf16[128,1024]{1,0:T(8,128)(2,1)}), bf16[2048,1024]{1,0:T(8,128)(2,1)}) %all-gather.22.cloned.1.call-update) | async-done | bytes 4194320 | tf_op jit(solution)/shard_map/all_gather | solution.py:148
  822.2 4.5 fusion.88
  826.8 72.4 %all-gather.20.cloned.1.call-done = bf16[2048,1024]{1,0:T(8,128)(2,1)} async-done(((bf16[128,1024]{1,0:T(8,128)(2,1)}), bf16[2048,1024]{1,0:T(8,128)(2,1)}) %all-gather.20.cloned.1.call-update) | async-done | bytes 4194320 | tf_op jit(solution)/shard_map/all_gather | solution.py:147
  899.2 3.8 fusion.89
  903.0 3.3 collective-permute-start
  908.3 6.0 fusion.155
  914.3 2.4 all-reduce
  916.7 59.5 %all-gather.24.cloned.1.call-done = bf16[2048,1024]{1,0:T(8,128)(2,1)} async-done(((bf16[128,1024]{1,0:T(8,128)(2,1)}), bf16[2048,1024]{1,0:T(8,128)(2,1)}) %all-gather.24.cloned.1.call-update) | async-done | bytes 4194320 | tf_op jit(solution)/shard_map/all_gather | solution.py:239
  976.2 4.0 fusion.98
  980.2 57.8 %all-gather.18.cloned.1.call-done = bf16[2048,512]{1,0:T(8,128)(2,1)} async-done(((bf16[128,512]{1,0:T(8,128)(2,1)}), bf16[2048,512]{1,0:T(8,128)(2,1)}) %all-gather.18.cloned.1.call-update) | async-done | bytes 2097168 | tf_op jit(solution)/shard_map/all_gather | solution.py:239
  1038.0 3.4 fusion.82
  1041.4 18.4 %all-reduce.3.cloned.1.call-done = bf16[256,2048]{1,0:T(8,128)(2,1)} async-done(((bf16[256,2048]{1,0:T(8,128)(2,1)}), bf16[256,2048]{1,0:T(8,128)(2,1)}) %all-reduce.3.cloned.1.call-update) | async-done | bytes 1048592 | tf_op jit(solution)/shard_map/psum | solution.py:245
  (284 shorter events, 135.6 us)
Async XLA Ops:
  6.5 66.7 %all-gather.12.cloned.1.call-start = ((), (), s32[]{:S(2)}) async-start(), calls=%async_computation | async-start | bytes 2228224 | tf_op jit(solution)/shard_map/all_gather | solution.py:145
  7.3 128.0 %all-gather.14.cloned.1.call-start = ((), (), s32[]{:S(2)}) async-start(), calls=%async_computation.1 | async-start | bytes 2228224 | tf_op jit(solution)/shard_map/all_gather | solution.py:146
  8.0 189.2 %all-gather.16.cloned.1.call-start = ((), (), s32[]{:S(2)}) async-start(), calls=%async_computation.2 | async-start | bytes 2228224 | tf_op jit(solution)/shard_map/all_gather | solution.py:144
  8.7 659.8 %all-gather.26.cloned.1.call-start = ((), (), s32[]{:S(2)}) async-start(), calls=%async_computation.8 | async-start | bytes 4456448 | tf_op jit(solution)/shard_map/all_gather | solution.py:17
  10.3 186.9 %copy-start.21 = (f32[256]{0:T(256)}, f32[256]{0:T(256)S(1)}, u32[]{:S(2)}) copy-start(f32[256]{0:T(256)S(1)} %add_rsqrt_fusion.1) | copy-start | bytes 3076
  204.4 27.5 %copy-start.9 = (f32[2,8,128,64]{2,0,3,1:T(2,128)}, f32[2,8,128,64]{2,0,3,1:T(2,128)S(1)}, u32[]{:S(2)}) copy-start(f32[2,8,128,64]{2,0,3,1:T(2,128)S(1)} %get-tuple-element.504) | copy-start | bytes 1572868 | tf_op jit(solution)/shard_map/while
  234.5 34.2 %copy-start.3 = (f32[8,128,64]{2,1,0:T(8,128)}, f32[8,128,64]{2,1,0:T(8,128)S(1)}, u32[]{:S(2)}) copy-start(f32[8,128,64]{2,1,0:T(8,128)S(1)} %copy.216) | copy-start | bytes 786436 | tf_op jit(solution)/shard_map/while
  317.8 34.3 %copy-start.5 = (f32[8,128,64]{2,1,0:T(8,128)S(1)}, f32[8,128,64]{2,1,0:T(8,128)}, u32[]{:S(2)}) copy-start(f32[8,128,64]{2,1,0:T(8,128)} %copy-done.3) | copy-start | bytes 786436 | tf_op jit(solution)/shard_map/while
  317.8 34.3 %copy-start.7 = (f32[8,128,64,1]{2,3,1,0:T(1,128)S(1)}, f32[8,128,64,1]{2,3,1,0:T(1,128)}, u32[]{:S(2)}) copy-start(f32[8,128,64,1]{2,3,1,0:T(1,128)} %copy.217) | copy-start | bytes 786436 | tf_op jit(solution)/shard_map/while
  386.7 4.8 copy-start.2
  387.9 4.2 copy-start.8
  395.2 27.5 %copy-start.9 = (f32[2,8,128,64]{2,0,3,1:T(2,128)}, f32[2,8,128,64]{2,0,3,1:T(2,128)S(1)}, u32[]{:S(2)}) copy-start(f32[2,8,128,64]{2,0,3,1:T(2,128)S(1)} %get-tuple-element.504) | copy-start | bytes 1572868 | tf_op jit(solution)/shard_map/while
  425.3 34.0 %copy-start.3 = (f32[8,128,64]{2,1,0:T(8,128)}, f32[8,128,64]{2,1,0:T(8,128)S(1)}, u32[]{:S(2)}) copy-start(f32[8,128,64]{2,1,0:T(8,128)S(1)} %copy.216) | copy-start | bytes 786436 | tf_op jit(solution)/shard_map/while
  508.5 34.3 %copy-start.5 = (f32[8,128,64]{2,1,0:T(8,128)S(1)}, f32[8,128,64]{2,1,0:T(8,128)}, u32[]{:S(2)}) copy-start(f32[8,128,64]{2,1,0:T(8,128)} %copy-done.3) | copy-start | bytes 786436 | tf_op jit(solution)/shard_map/while
  508.5 34.3 %copy-start.7 = (f32[8,128,64,1]{2,3,1,0:T(1,128)S(1)}, f32[8,128,64,1]{2,3,1,0:T(1,128)}, u32[]{:S(2)}) copy-start(f32[8,128,64,1]{2,3,1,0:T(1,128)} %copy.217) | copy-start | bytes 786436 | tf_op jit(solution)/shard_map/while
  577.4 4.8 copy-start.2
  592.1 5.6 copy-start.17
  594.0 151.4 %all-gather.28.cloned.1.call-start = ((), (), s32[]{:S(2)}) async-start(), calls=%async_computation.9 | async-start | bytes 4456448 | tf_op jit(solution)/shard_map/all_gather | solution.py:17
  594.9 227.3 %all-gather.22.cloned.1.call-start = ((), (), s32[]{:S(2)}) async-start(), calls=%async_computation.5 | async-start | bytes 4456448 | tf_op jit(solution)/shard_map/all_gather | solution.py:148
  595.5 303.7 %all-gather.20.cloned.1.call-start = ((), (), s32[]{:S(2)}) async-start(), calls=%async_computation.4 | async-start | bytes 4456448 | tf_op jit(solution)/shard_map/all_gather | solution.py:147
  596.2 380.0 %all-gather.24.cloned.1.call-start = ((), (), s32[]{:S(2)}) async-start(), calls=%async_computation.6 | async-start | bytes 4456448 | tf_op jit(solution)/shard_map/all_gather | solution.py:239
  597.0 441.0 %all-gather.18.cloned.1.call-start = ((), (), s32[]{:S(2)}) async-start(), calls=%async_computation.3 | async-start | bytes 2228224 | tf_op jit(solution)/shard_map/all_gather | solution.py:239
  597.7 462.1 %all-reduce.3.cloned.1.call-start = ((), (), s32[]{:S(2)}) async-start(), calls=%async_computation.7 | async-start | bytes 2097152 | tf_op jit(solution)/shard_map/psum | solution.py:245
  745.4 76.9 %copy-start.12 = (bf16[256,2048]{1,0:T(8,128)(2,1)S(1)}, bf16[256,2048]{1,0:T(8,128)(2,1)}, u32[]{:S(2)}) copy-start(bf16[256,2048]{1,0:T(8,128)(2,1)} %param.24) | copy-start | bytes 3145732
  745.4 76.9 %copy-start.22 = (f32[256]{0:T(256)S(1)}, f32[256]{0:T(256)}, u32[]{:S(2)}) copy-start(f32[256]{0:T(256)} %copy-done.21) | copy-start | bytes 3076
  745.4 76.9 %copy-start.25 = (f32[2048]{0:T(1024)S(1)}, f32[2048]{0:T(1024)}, u32[]{:S(2)}) copy-start(f32[2048]{0:T(1024)} %param.25) | copy-start | bytes 24580
  826.8 79.6 %copy-start.13 = (f32[2,8,128,64]{2,3,0,1:T(8,128)S(1)}, f32[2,8,128,64]{2,3,0,1:T(8,128)}, u32[]{:S(2)}) copy-start(f32[2,8,128,64]{2,3,0,1:T(8,128)} %get-tuple-element.159) | copy-start | bytes 1572868
  826.8 79.6 %copy-start.16 = (f32[2,8,128,64]{2,3,0,1:T(8,128)S(1)}, f32[2,8,128,64]{2,3,0,1:T(8,128)}, u32[]{:S(2)}) copy-start(f32[2,8,128,64]{2,3,0,1:T(8,128)} %get-tuple-element.163) | copy-start | bytes 1572868
  903.0 4.6 copy-start.20
  903.0 5.2 collective-permute-start
  907.1 69.1 %copy-start.26 = (f32[1024]{0:T(1024)S(1)}, f32[1024]{0:T(1024)}, u32[]{:S(2)}) copy-start(f32[1024]{0:T(1024)} %param.41) | copy-start | bytes 12292
  1038.0 24.1 %copy-start.1 = (bf16[2048,128]{1,0:T(8,128)(2,1)S(1)}, bf16[2048,128]{1,0:T(8,128)(2,1)}, u32[]{:S(2)}) copy-start(bf16[2048,128]{1,0:T(8,128)(2,1)} %param.35) | copy-start | bytes 1572868
  (18 other events, 36.1 us)
Sparse Core Ops, SparseCore 0:
  10.1 63.0 all-gather.11
  76.0 59.1 all-gather.13
  138.0 59.1 all-gather.15
  594.1 74.3 all-gather.25
  671.1 74.1 all-gather.27
  748.0 74.1 all-gather.21
  825.0 74.1 all-gather.19
  902.0 74.1 all-gather.23
  979.0 58.9 all-gather.17
  1041.5 18.1 all-reduce.2
where the time goes:
time: 1080 us; the launch traced here: 1070 us
  waiting for transfers between devices  567 us (52%)
  matrix products  365 us (34%)
  other arithmetic  59.7 us (6%)
  local copies, waits for them, and re-layouts  48.4 us (4%)
  between operations  14.4 us (1%)
    dot_general x8, matrix products, paired(): jnp.einsum('htc,htsc,hsc->hts', left, pair_decay, right, precision=HIGHEST)  267 us
    all_gather x2, waiting for transfers between devices, entering(): everything = jax.tree.map(lambda part: lax.all_gather(part, axis), x)  147 us
    all_gather x2, waiting for transfers between devices, body(): lax.all_gather((attention_output_matrix, convolution_output_matrix), 'sp'...  117 us
    all_gather x1, waiting for transfers between devices, body(): lax.all_gather(convolution_value_matrix, 'sp', axis=0, tiled=True)  72.4 us
    dot_general x67, matrix products, exact_mul(): return jnp.einsum(form, left, right, precision=HIGHEST)  70.9 us
    all_gather x1, waiting for transfers between devices, body(): lax.all_gather(query_matrix, 'sp', axis=0, tiled=True)  59.1 us
    all_gather x1, waiting for transfers between devices, body(): lax.all_gather(value_matrix, 'sp', axis=0, tiled=True)  58.1 us
    all_gather x1, waiting for transfers between devices, body(): lax.all_gather(key_matrix, 'sp', axis=0, tiled=True)  55.9 us
  transfers between devices with their start and end apart: 11, of which 11 were waited for; matrix products, arithmetic and copies ran while one was open for 7% of the time, Pallas kernels for 0%

commit v1 on v0

--- a/solution.py
+++ b/solution.py
@@ -10,6 +10,19 @@
 GROUP_EPSILON = 0.00064
 LAYER_EPSILON = 1e-05
 UNIT_EPSILON = 1e-06
+
+
+def follow_the_rows(base_x):
+    current_value = jnp.concatenate(
+        lax.all_to_all(
+            jnp.stack([base_x for _ in range(lax.axis_size("sp"))]),
+            concat_axis=0,
+            axis_name="sp",
+            split_axis=0,
+        ),
+        axis=0,
+    )
+    return current_value
 
 
 def entering(x, axis, combine, identity):
@@ -141,7 +154,7 @@
         * input_norm_gain
     ).astype(jnp.bfloat16)
     pieces = (
-        lax.all_gather(query_matrix, "sp", axis=0, tiled=True),
+        follow_the_rows(query_matrix),
         lax.all_gather(key_matrix, "sp", axis=0, tiled=True),
         lax.all_gather(value_matrix, "sp", axis=0, tiled=True),
         lax.all_gather(convolution_value_matrix, "sp", axis=0, tiled=True),

time: 1080 us -> 1030 us (0.954)
  waiting for transfers between devices: 567 us -> 499 us
    all_gather x1 -> x0, waiting for transfers between devices: 59.1 us -> none  [body(): lax.all_gather(query_matrix, 'sp', axis=0, tiled=True)]
  transfers between devices with their start and end apart: 11 -> 11, of which waited for: 11 -> 10; matrix products, arithmetic and copies ran while one was open for 7% -> 9% of each run, Pallas kernels for 0% -> 0%
where the time goes in v1:
time: 1030 us
  waiting for transfers between devices  499 us (48%)
  matrix products  369 us (36%)
  other arithmetic  62.7 us (6%)
  local copies, waits for them, and re-layouts  58.3 us (6%)
  between operations  13.8 us (1%)
  starting transfers between devices  12.1 us (1%)
    dot_general x8, matrix products, paired(): jnp.einsum('htc,htsc,hsc->hts', left, pair_decay, right, precision=HIGHEST)  267 us
    all_gather x2, waiting for transfers between devices, entering(): everything = jax.tree.map(lambda part: lax.all_gather(part, axis), x)  145 us
    all_gather x2, waiting for transfers between devices, body(): lax.all_gather((attention_output_matrix, convolution_output_matrix), 'sp'...  117 us
    dot_general x67, matrix products, exact_mul(): return jnp.einsum(form, left, right, precision=HIGHEST)  72.7 us
    all_gather x1, waiting for transfers between devices, body(): lax.all_gather(convolution_value_matrix, 'sp', axis=0, tiled=True)  72.3 us
    all_gather x1, waiting for transfers between devices, body(): lax.all_gather(key_matrix, 'sp', axis=0, tiled=True)  58.9 us
    all_gather x1, waiting for transfers between devices, body(): lax.all_gather(value_matrix, 'sp', axis=0, tiled=True)  49.5 us
    another operation x2, other arithmetic, block_update(): log_gain = jnp.cumsum(logdec_blk, axis=1)  46.6 us
  transfers between devices with their start and end apart: 11, of which 10 were waited for; matrix products, arithmetic and copies ran while one was open for 9% of the time, Pallas kernels for 0%

profile of v1, /device:TPU:0, one launch (start us, length us, event | category | flops | bytes accessed | tf_op | source)
XLA Modules:
  0.0 1025.8 jit_solution(3166189606075823311)
XLA Ops:
  10.0 8.5 all-to-all-start
  30.5 58.9 %all-gather.11.cloned.1.call-done = bf16[2048,512]{1,0:T(8,128)(2,1)} async-done(((bf16[128,512]{1,0:T(8,128)(2,1)}), bf16[2048,512]{1,0:T(8,128)(2,1)}) %all-gather.11.cloned.1.call-update) | async-done | bytes 2097168 | tf_op jit(solution)/shard_map/all_gather | solution.py:158
  89.3 3.4 fusion.149
  98.0 4.1 copy.189
  102.1 49.5 %all-gather.13.cloned.1.call-done = bf16[2048,512]{1,0:T(8,128)(2,1)} async-done(((bf16[128,512]{1,0:T(8,128)(2,1)}), bf16[2048,512]{1,0:T(8,128)(2,1)}) %all-gather.13.cloned.1.call-update) | async-done | bytes 2097168 | tf_op jit(solution)/shard_map/all_gather | solution.py:159
  151.5 2.8 fusion.160
  155.4 3.1 convolution_bitcast_fusion.5
  161.9 387.5 %while.31 = (s32[]{:T(128)}, f32[8,64,64]{1,2,0:T(8,128)}, f32[8,64,64]{1,2,0:T(8,128)S(1)}, f32[2,8,128,64]{2,3,0,1:T(8,128)}, f32[2,8,128,64]{2,3,0,1:T(8,128)...) while((s32[]{:T(128)}, f32[8,64,64]{1,2,0:T(8,128)}, ...), condition=%wide.region_6.7_spmd.clone, body=%wide.region_2.6_spmd.clone.sunk | while | flops 3836598272 | bytes 48321828 | solution.py:215
  163.4 23.3 %fusion.369 = f32[8,128,64]{2,0,1:T(8,128)S(1)} fusion(f32[8,128,64]{2,0,1:T(8,128)S(1)} %copy.253), kind=kOutput, calls=%fused_computation.246.clone.1 | output fusion | flops 8323072 | bytes 524288 | tf_op jit(solution)/shard_map/while/body/eval_jaxpr/jit(cumsum)/reduce_window_sum | solution.py:69
  192.8 32.8 %fusion.371 = f32[8,128,1,128]{3,2,1,0:T(1,128)S(1)} fusion(f32[8,128,64,1]{2,3,1,0:T(1,128)} %copy.252, f32[8,128,64]{1,2,0:T(8,128)S(1)} %bitcast.408, f32[8,128,64]{1,2,0:T(8,128)S(1)} %copy.254, f32[8,128,64]{2,1,0:T(8,128)S(1)} %copy.255, pred[128,128]{1,0:T(8,128)(4,1)S(1)} %iota_compare_fusion.5), kind=kOutput, calls=%fused_computation.6.clone.1 | convolution fusion | flops 125829120 | bytes 1589248 | tf_op jit(solution)/shard_map/while/body/eval_jaxpr/htc,htsc,hsc->hts/dot_general | solution.py:80
  233.6 35.6 %fusion.382 = f32[8,128,1,128]{3,2,1,0:T(1,128)S(1)} fusion(f32[8,128,64,1]{2,3,1,0:T(1,128)S(1)} %copy-done.5, f32[8,128,64]{1,2,0:T(8,128)S(1)} %bitcast.417, f32[8,128,64]{1,2,0:T(8,128)S(1)} %copy.254, f32[8,128,64]{2,1,0:T(8,128)S(1)} %copy-done.3, pred[128,128]{1,0:T(8,128)(4,1)S(1)} %iota_compare_fusion.5), kind=kOutput, calls=%fused_computation.2.clone.1 | convolution fusion | flops 125829120 | bytes 1589248 | tf_op jit(solution)/shard_map/while/body/eval_jaxpr/htc,htsc,hsc->hts/dot_general | solution.py:80
  273.8 33.0 %fusion.387 = f32[8,128,1,128]{3,2,1,0:T(1,128)S(1)} fusion(f32[8,128,64,1]{2,3,1,0:T(1,128)} %copy.256, f32[8,128,64]{1,2,0:T(8,128)S(1)} %bitcast.410, f32[8,128,64]{1,2,0:T(8,128)S(1)} %copy.254, f32[8,128,64]{2,1,0:T(8,128)} %copy-done.2, pred[128,128]{1,0:T(8,128)(4,1)S(1)} %iota_compare_fusion.5), kind=kOutput, calls=%fused_computation.4.clone.1 | convolution fusion | flops 125829120 | bytes 1589248 | tf_op jit(solution)/shard_map/while/body/eval_jaxpr/htc,htsc,hsc->hts/dot_general | solution.py:80
  308.1 31.9 %fusion.389 = f32[8,128,1,128]{3,2,1,0:T(1,128)S(1)} fusion(f32[8,128,64,1]{2,3,1,0:T(1,128)S(1)} %copy-done.6, f32[8,128,64]{1,2,0:T(8,128)S(1)} %bitcast.418, f32[8,128,64]{1,2,0:T(8,128)S(1)} %copy.254, f32[8,128,64]{2,1,0:T(8,128)S(1)} %copy-done.4, pred[128,128]{1,0:T(8,128)(4,1)S(1)} %iota_compare_fusion.5), kind=kOutput, calls=%fused_computation.clone.2 | convolution fusion | flops 125829120 | bytes 1589248 | tf_op jit(solution)/shard_map/while/body/eval_jaxpr/htc,htsc,hsc->hts/dot_general | solution.py:80
  354.0 23.3 %fusion.369 = f32[8,128,64]{2,0,1:T(8,128)S(1)} fusion(f32[8,128,64]{2,0,1:T(8,128)S(1)} %copy.253), kind=kOutput, calls=%fused_computation.246.clone.1 | output fusion | flops 8323072 | bytes 524288 | tf_op jit(solution)/shard_map/while/body/eval_jaxpr/jit(cumsum)/reduce_window_sum | solution.py:69
  383.4 32.8 %fusion.371 = f32[8,128,1,128]{3,2,1,0:T(1,128)S(1)} fusion(f32[8,128,64,1]{2,3,1,0:T(1,128)} %copy.252, f32[8,128,64]{1,2,0:T(8,128)S(1)} %bitcast.408, f32[8,128,64]{1,2,0:T(8,128)S(1)} %copy.254, f32[8,128,64]{2,1,0:T(8,128)S(1)} %copy.255, pred[128,128]{1,0:T(8,128)(4,1)S(1)} %iota_compare_fusion.5), kind=kOutput, calls=%fused_computation.6.clone.1 | convolution fusion | flops 125829120 | bytes 1589248 | tf_op jit(solution)/shard_map/while/body/eval_jaxpr/htc,htsc,hsc->hts/dot_general | solution.py:80
  424.2 35.6 %fusion.382 = f32[8,128,1,128]{3,2,1,0:T(1,128)S(1)} fusion(f32[8,128,64,1]{2,3,1,0:T(1,128)S(1)} %copy-done.5, f32[8,128,64]{1,2,0:T(8,128)S(1)} %bitcast.417, f32[8,128,64]{1,2,0:T(8,128)S(1)} %copy.254, f32[8,128,64]{2,1,0:T(8,128)S(1)} %copy-done.3, pred[128,128]{1,0:T(8,128)(4,1)S(1)} %iota_compare_fusion.5), kind=kOutput, calls=%fused_computation.2.clone.1 | convolution fusion | flops 125829120 | bytes 1589248 | tf_op jit(solution)/shard_map/while/body/eval_jaxpr/htc,htsc,hsc->hts/dot_general | solution.py:80
  464.4 33.0 %fusion.387 = f32[8,128,1,128]{3,2,1,0:T(1,128)S(1)} fusion(f32[8,128,64,1]{2,3,1,0:T(1,128)} %copy.256, f32[8,128,64]{1,2,0:T(8,128)S(1)} %bitcast.410, f32[8,128,64]{1,2,0:T(8,128)S(1)} %copy.254, f32[8,128,64]{2,1,0:T(8,128)} %copy-done.2, pred[128,128]{1,0:T(8,128)(4,1)S(1)} %iota_compare_fusion.5), kind=kOutput, calls=%fused_computation.4.clone.1 | convolution fusion | flops 125829120 | bytes 1589248 | tf_op jit(solution)/shard_map/while/body/eval_jaxpr/htc,htsc,hsc->hts/dot_general | solution.py:80
  498.6 31.9 %fusion.389 = f32[8,128,1,128]{3,2,1,0:T(1,128)S(1)} fusion(f32[8,128,64,1]{2,3,1,0:T(1,128)S(1)} %copy-done.6, f32[8,128,64]{1,2,0:T(8,128)S(1)} %bitcast.418, f32[8,128,64]{1,2,0:T(8,128)S(1)} %copy.254, f32[8,128,64]{2,1,0:T(8,128)S(1)} %copy-done.4, pred[128,128]{1,0:T(8,128)(4,1)S(1)} %iota_compare_fusion.5), kind=kOutput, calls=%fused_computation.clone.2 | convolution fusion | flops 125829120 | bytes 1589248 | tf_op jit(solution)/shard_map/while/body/eval_jaxpr/htc,htsc,hsc->hts/dot_general | solution.py:80
  557.3 68.5 %all-gather.23.cloned.1.call-done = f32[128,64,64]{2,1,0:T(8,128)} async-done(((f32[8,64,64]{2,1,0:T(8,128)}), f32[128,64,64]{2,1,0:T(8,128)}) %all-gather.23.cloned.1.call-update) | async-done | bytes 2097168 | tf_op jit(solution)/shard_map/all_gather | solution.py:30
  625.8 76.8 %all-gather.25.cloned.1.call-done = f32[128,64,64]{2,1,0:T(8,128)} async-done(((f32[8,64,64]{2,1,0:T(8,128)}), f32[128,64,64]{2,1,0:T(8,128)}) %all-gather.25.cloned.1.call-update) | async-done | bytes 2097168 | tf_op jit(solution)/shard_map/all_gather | solution.py:30
  702.6 43.6 %while.32 = (s32[]{:T(128)}, f32[8,64,64]{1,2,0:T(8,128)S(1)}, s32[]{:T(128)}, f32[16,8,64,64]{3,2,1,0:T(8,128)}, f32[16,8,64,64]{3,2,1,0:T(8,128)}, /*index=5*/s32[]{:T(128)}, s32[]{:T(128)}) while((s32[]{:T(128)}, f32[8,64,64]{1,2,0:T(8,128)S(1)}, s32[]{:T(128)}, f32[16,8,64,64]{3,2,1,0:T(8,128)}, f32[16,8,64,64]{3,2,1,0:T(8,128)}, ...), condition=%wide.region_8.9_spmd.clone, body=%wide.region_7.8_spmd.clone.sunk | while | flops 25296900 | bytes 1968227 | solution.py:40
  746.2 33.2 %all-gather.19.cloned.1.call-done = bf16[2048,1024]{1,0:T(8,128)(2,1)} async-done(((bf16[128,1024]{1,0:T(8,128)(2,1)}), bf16[2048,1024]{1,0:T(8,128)(2,1)}) %all-gather.19.cloned.1.call-update) | async-done | bytes 4194320 | tf_op jit(solution)/shard_map/all_gather | solution.py:161
  779.4 4.5 fusion.91
  783.9 72.3 %all-gather.17.cloned.1.call-done = bf16[2048,1024]{1,0:T(8,128)(2,1)} async-done(((bf16[128,1024]{1,0:T(8,128)(2,1)}), bf16[2048,1024]{1,0:T(8,128)(2,1)}) %all-gather.17.cloned.1.call-update) | async-done | bytes 4194320 | tf_op jit(solution)/shard_map/all_gather | solution.py:160
  856.3 3.7 fusion.92
  860.1 3.4 collective-permute-start
  865.3 6.0 fusion.146
  873.8 59.5 %all-gather.21.cloned.1.call-done = bf16[2048,1024]{1,0:T(8,128)(2,1)} async-done(((bf16[128,1024]{1,0:T(8,128)(2,1)}), bf16[2048,1024]{1,0:T(8,128)(2,1)}) %all-gather.21.cloned.1.call-update) | async-done | bytes 4194320 | tf_op jit(solution)/shard_map/all_gather | solution.py:252
  933.3 4.0 fusion.101
  937.3 57.7 %all-gather.15.cloned.1.call-done = bf16[2048,512]{1,0:T(8,128)(2,1)} async-done(((bf16[128,512]{1,0:T(8,128)(2,1)}), bf16[2048,512]{1,0:T(8,128)(2,1)}) %all-gather.15.cloned.1.call-update) | async-done | bytes 2097168 | tf_op jit(solution)/shard_map/all_gather | solution.py:252
  995.1 3.3 fusion.85
  998.4 18.4 %all-reduce.3.cloned.1.call-done = bf16[256,2048]{1,0:T(8,128)(2,1)} async-done(((bf16[256,2048]{1,0:T(8,128)(2,1)}), bf16[256,2048]{1,0:T(8,128)(2,1)}) %all-reduce.3.cloned.1.call-update) | async-done | bytes 1048592 | tf_op jit(solution)/shard_map/psum | solution.py:258
  (259 shorter events, 148.5 us)
Async XLA Ops:
  6.5 16.9 %copy-start = (bf16[2048,128]{1,0:T(8,128)(2,1)S(1)}, bf16[2048,128]{1,0:T(8,128)(2,1)}, u32[]{:S(2)}) copy-start(bf16[2048,128]{1,0:T(8,128)(2,1)} %param.35) | copy-start | bytes 1572868
  6.5 14.3 %copy-start.12 = (f32[2048]{0:T(1024)S(1)}, f32[2048]{0:T(1024)}, u32[]{:S(2)}) copy-start(f32[2048]{0:T(1024)} %param.25) | copy-start | bytes 24580
  6.5 82.8 %all-gather.11.cloned.1.call-start = ((), (), s32[]{:S(2)}) async-start(), calls=%async_computation.1 | async-start | bytes 2228224 | tf_op jit(solution)/shard_map/all_gather | solution.py:158
  10.0 13.4 %copy-start.16 = (bf16[128,512]{1,0:T(8,128)(2,1)S(1)}, bf16[128,512]{1,0:T(8,128)(2,1)}, u32[]{:S(2)}) copy-start(bf16[128,512]{1,0:T(8,128)(2,1)} %param.36) | copy-start | bytes 393220
  10.0 13.4 %copy-start.18 = (f32[512]{0:T(512)S(1)}, f32[512]{0:T(512)}, u32[]{:S(2)}) copy-start(f32[512]{0:T(512)} %param.34) | copy-start | bytes 6148
  10.0 85.3 %all-to-all-start = ((bf16[16,128,512]{1,2,0:T(8,128)(2,1)}), bf16[16,128,512]{1,2,0:T(8,128)(2,1)S(1)}, u32[]{:S(2)}, u32[]{:S(2)}) async-start(bf16[16,128,512]{1,2,0:T(8,128)(2,1)} %stack.2), calls=%async_computation | async-start | bytes 4194304 | tf_op jit(solution)/shard_map/all_to_all | solution.py:17
  18.5 133.0 %all-gather.13.cloned.1.call-start = ((), (), s32[]{:S(2)}) async-start(), calls=%async_computation.2 | async-start | bytes 2228224 | tf_op jit(solution)/shard_map/all_gather | solution.py:159
  19.3 606.5 %all-gather.23.cloned.1.call-start = ((), (), s32[]{:S(2)}) async-start(), calls=%async_computation.8 | async-start | bytes 4456448 | tf_op jit(solution)/shard_map/all_gather | solution.py:30
  20.9 5.7 copy-start.19
  25.3 4.1 copy-start.13
  25.3 4.1 copy-start.14
  98.0 57.5 %copy-start.7 = (bf16[256,2048]{1,0:T(8,128)(2,1)S(1)}, bf16[256,2048]{1,0:T(8,128)(2,1)}, u32[]{:S(2)}) copy-start(bf16[256,2048]{1,0:T(8,128)(2,1)} %fusion.88) | copy-start | bytes 3145732
  102.1 56.6 %copy-start.9 = (f32[2,128,8,64]{1,0,3,2:T(2,128)S(1)}, f32[2,128,8,64]{1,0,3,2:T(2,128)}, u32[]{:S(2)}) copy-start(f32[2,128,8,64]{1,0,3,2:T(2,128)} %reshape.138) | copy-start | bytes 1572868
  191.8 33.9 %copy-start.2 = (f32[8,128,64]{2,1,0:T(8,128)}, f32[8,128,64]{2,1,0:T(8,128)S(1)}, u32[]{:S(2)}) copy-start(f32[8,128,64]{2,1,0:T(8,128)S(1)} %copy.255) | copy-start | bytes 786436 | tf_op jit(solution)/shard_map/while
  273.8 34.2 %copy-start.4 = (f32[8,128,64]{2,1,0:T(8,128)S(1)}, f32[8,128,64]{2,1,0:T(8,128)}, u32[]{:S(2)}) copy-start(f32[8,128,64]{2,1,0:T(8,128)} %copy-done.2) | copy-start | bytes 786436 | tf_op jit(solution)/shard_map/while
  273.8 34.2 %copy-start.6 = (f32[8,128,64,1]{2,3,1,0:T(1,128)S(1)}, f32[8,128,64,1]{2,3,1,0:T(1,128)}, u32[]{:S(2)}) copy-start(f32[8,128,64,1]{2,3,1,0:T(1,128)} %copy.256) | copy-start | bytes 786436 | tf_op jit(solution)/shard_map/while
  382.3 33.9 %copy-start.2 = (f32[8,128,64]{2,1,0:T(8,128)}, f32[8,128,64]{2,1,0:T(8,128)S(1)}, u32[]{:S(2)}) copy-start(f32[8,128,64]{2,1,0:T(8,128)S(1)} %copy.255) | copy-start | bytes 786436 | tf_op jit(solution)/shard_map/while
  464.4 34.2 %copy-start.4 = (f32[8,128,64]{2,1,0:T(8,128)S(1)}, f32[8,128,64]{2,1,0:T(8,128)}, u32[]{:S(2)}) copy-start(f32[8,128,64]{2,1,0:T(8,128)} %copy-done.2) | copy-start | bytes 786436 | tf_op jit(solution)/shard_map/while
  464.4 34.2 %copy-start.6 = (f32[8,128,64,1]{2,3,1,0:T(1,128)S(1)}, f32[8,128,64,1]{2,3,1,0:T(1,128)}, u32[]{:S(2)}) copy-start(f32[8,128,64,1]{2,3,1,0:T(1,128)} %copy.256) | copy-start | bytes 786436 | tf_op jit(solution)/shard_map/while
  551.2 151.4 %all-gather.25.cloned.1.call-start = ((), (), s32[]{:S(2)}) async-start(), calls=%async_computation.9 | async-start | bytes 4456448 | tf_op jit(solution)/shard_map/all_gather | solution.py:30
  552.1 227.3 %all-gather.19.cloned.1.call-start = ((), (), s32[]{:S(2)}) async-start(), calls=%async_computation.5 | async-start | bytes 4456448 | tf_op jit(solution)/shard_map/all_gather | solution.py:161
  552.7 303.6 %all-gather.17.cloned.1.call-start = ((), (), s32[]{:S(2)}) async-start(), calls=%async_computation.4 | async-start | bytes 4456448 | tf_op jit(solution)/shard_map/all_gather | solution.py:160
  553.3 380.0 %all-gather.21.cloned.1.call-start = ((), (), s32[]{:S(2)}) async-start(), calls=%async_computation.6 | async-start | bytes 4456448 | tf_op jit(solution)/shard_map/all_gather | solution.py:252
  554.1 441.0 %all-gather.15.cloned.1.call-start = ((), (), s32[]{:S(2)}) async-start(), calls=%async_computation.3 | async-start | bytes 2228224 | tf_op jit(solution)/shard_map/all_gather | solution.py:252
  554.8 462.0 %all-reduce.3.cloned.1.call-start = ((), (), s32[]{:S(2)}) async-start(), calls=%async_computation.7 | async-start | bytes 2097152 | tf_op jit(solution)/shard_map/psum | solution.py:258
  702.6 76.8 %copy-start.8 = (bf16[256,2048]{1,0:T(8,128)(2,1)S(1)}, bf16[256,2048]{1,0:T(8,128)(2,1)}, u32[]{:S(2)}) copy-start(bf16[256,2048]{1,0:T(8,128)(2,1)} %fusion.88) | copy-start | bytes 3145732
  783.9 79.5 %copy-start.10 = (f32[2,8,128,64]{2,3,0,1:T(8,128)S(1)}, f32[2,8,128,64]{2,3,0,1:T(8,128)}, u32[]{:S(2)}) copy-start(f32[2,8,128,64]{2,3,0,1:T(8,128)} %get-tuple-element.159) | copy-start | bytes 1572868
  783.9 79.5 %copy-start.11 = (f32[2,8,128,64]{2,3,0,1:T(8,128)S(1)}, f32[2,8,128,64]{2,3,0,1:T(8,128)}, u32[]{:S(2)}) copy-start(f32[2,8,128,64]{2,3,0,1:T(8,128)} %get-tuple-element.163) | copy-start | bytes 1572868
  783.9 80.7 %copy-start.15 = (f32[512]{0:T(512)S(1)}, f32[512]{0:T(512)}, u32[]{:S(2)}) copy-start(f32[512]{0:T(512)} %param.39) | copy-start | bytes 6148
  860.0 73.3 %copy-start.17 = (f32[1024]{0:T(1024)S(1)}, f32[1024]{0:T(1024)}, u32[]{:S(2)}) copy-start(f32[1024]{0:T(1024)} %param.41) | copy-start | bytes 12292
  860.1 5.2 collective-permute-start
  933.3 85.8 %copy-start.1 = (bf16[2048,128]{1,0:T(8,128)(2,1)S(1)}, bf16[2048,128]{1,0:T(8,128)(2,1)}, u32[]{:S(2)}) copy-start(bf16[2048,128]{1,0:T(8,128)(2,1)} %param.35) | copy-start | bytes 1572868
  (4 other events, 13.4 us)
Sparse Core Ops, SparseCore 0:
  10.1 79.1 all-gather.10
  92.1 59.3 all-gather.12
  551.3 74.3 all-gather.22
  628.4 74.1 all-gather.24
  705.2 74.1 all-gather.18
  782.1 74.1 all-gather.16
  859.1 74.1 all-gather.20
  936.1 58.9 all-gather.14
  998.5 18.1 all-reduce.2
